TPU v7x, 32 devices: a whole 2x2x4 slice. The times are simulated.
32 devices in a mesh: ep: 8 (over z, x), tp: 4 (over y, core).
Axes of the slice: x: 2, y: 2, z: 4, core: 2. Of those that a mesh axis runs over, the one named last changes fastest.
Arguments:
- residual: bfloat16 [512, 4096], P('ep', 'tp'), may hold values from -64 to 64
- routes: int32 [512, 2], P('ep'), may hold values from 0 to 7, all different within a row; in each aligned block of 64 rows (0 to 63, 64 to 127, ...) at most 32 rows name the same one
- route_weights: float32 [512, 2], P('ep'), may hold values from 0.2 to 1
- state_prev: float32 [512, 2, 64, 64], P('ep', None, 'tp'), may hold values from -6 to 6
- mix_gain: float32 [4096], replicated, may hold values from 0.1 to 1.9
- ffn_gain: float32 [4096], replicated, may hold values from 0.1 to 1.9
- w_in: bfloat16 [4096, 1024], P(None, 'tp'), may hold values from -0.09375 to 0.09375
- decay_rate: float32 [64, 64], P('tp'), may hold values from 0.5 to 8
- rotation: float32 [64, 64], P('tp'), may hold values from 0 to 200
- log_step: float32 [64], P('tp'), may hold values from -3.9 to -1.2
- in_re: float32 [64, 64, 16], P('tp'), may hold values from -1 to 1
- in_im: float32 [64, 64, 16], P('tp'), may hold values from -1 to 1
- read_re: float32 [64, 16, 64], P('tp'), may hold values from -0.5 to 0.5
- read_im: float32 [64, 16, 64], P('tp'), may hold values from -0.5 to 0.5
- skip_gain: float32 [64, 16], P('tp'), may hold values from -4 to 4
- w_glu: bfloat16 [1024, 1024], P(None, 'tp'), may hold values from -0.1875 to 0.1875
- w_out: bfloat16 [1024, 4096], P('tp'), may hold values from -0.1875 to 0.1875
- w_gate: bfloat16 [8, 4096, 5632], P('ep', None, 'tp'), may hold values from -0.09375 to 0.09375
- w_up: bfloat16 [8, 4096, 5632], P('ep', None, 'tp'), may hold values from -0.09375 to 0.09375
- w_down: bfloat16 [8, 5632, 4096], P('ep', 'tp'), may hold values from -0.078125 to 0.078125
Outputs:
- layer_out: bfloat16 [512, 4096], P('ep', 'tp')
- state_next: float32 [512, 2, 64, 64], P('ep', None, 'tp')
Inputs may be any that keep to these rules, and one draw needn't show every extreme that they name: `routes`: each row names 2 different experts. In each aligned block of 64 rows (the rows of one index of ep) no expert is named more than 32 times, a bound that some block reaches.
All inputs are finite; a program needn't handle non-finite values.
Results may differ from a plain program's by a relative error of at most 0.012.
Values may be sent and summed in bfloat16 or wider, within the bound.
No kernel may reach another device: no remote copies, remote signals or barrier semaphores. Data moves between devices by JAX's collectives and lax.ppermute only.
A program may use at most 128 MiB of HBM per device.

v0:
```python
import jax
import jax.numpy as jnp
from jax import lax
from jax.sharding import PartitionSpec as P

GROUP_CH = 16
TOPK = 2
epsilon = 1e-06
highest = lax.Precision.HIGHEST


def state_mixer(
    u_in, state_prev, decay_rate, rotation, log_step, in_re, in_im, read_re, read_im, skip_gain
):
    batch_rows = u_in.shape[0]
    groups = decay_rate.shape[0]
    grouped = u_in.astype(jnp.float32).reshape(batch_rows, groups, GROUP_CH)
    step_size = jnp.exp(log_step)[:, None]
    real_part = -decay_rate
    magnitude = jnp.exp(real_part * step_size)
    decay_re = magnitude * jnp.cos(rotation * step_size)
    decay_im = magnitude * jnp.sin(rotation * step_size)
    denominator = real_part * real_part + rotation * rotation
    lift_re = ((decay_re - 1.0) * real_part + decay_im * rotation) / denominator
    lift_im = (decay_im * real_part - (decay_re - 1.0) * rotation) / denominator
    map_re = lift_re[..., None] * in_re - lift_im[..., None] * in_im
    map_im = lift_re[..., None] * in_im + lift_im[..., None] * in_re
    drive_re = jnp.einsum("gph,bgh->bgp", map_re, grouped, precision=highest)
    drive_im = jnp.einsum("gph,bgh->bgp", map_im, grouped, precision=highest)
    old_re = state_prev[:, 0]
    old_im = state_prev[:, 1]
    new_re = decay_re * old_re - decay_im * old_im + drive_re
    new_im = decay_re * old_im + decay_im * old_re + drive_im
    output = (
        jnp.einsum("ghp,bgp->bgh", read_re, new_re, precision=highest)
        - jnp.einsum("ghp,bgp->bgh", read_im, new_im, precision=highest)
        + skip_gain * grouped
    )
    return (jax.nn.gelu(output.reshape(batch_rows, -1)), jnp.stack([new_re, new_im], axis=1))


def per_device(
    residual,
    routes,
    route_weights,
    state_prev,
    mix_gain,
    ffn_gain,
    w_in,
    decay_rate,
    rotation,
    log_step,
    in_re,
    in_im,
    read_re,
    read_im,
    skip_gain,
    w_glu,
    w_out,
    w_gate,
    w_up,
    w_down,
):
    shard_width = residual.shape[1]
    full_width = shard_width * lax.axis_size("tp")
    tp_place = lax.axis_index("tp")
    experts_all = lax.axis_size("ep")
    seq_rows = residual.shape[0]
    capacity = 2 * seq_rows * TOPK // experts_all
    source = residual.astype(jnp.float32)
    squares = lax.psum(jnp.sum(source * source, axis=1), "tp")
    own_gain = lax.dynamic_slice_in_dim(mix_gain, tp_place * shard_width, shard_width)
    scale_rows = lax.rsqrt(squares / full_width + epsilon)[:, None]
    outgoing = (source * scale_rows * own_gain).astype(jnp.bfloat16)
    gathered = lax.all_gather(outgoing, "tp", axis=1, tiled=True)
    u_in = jnp.dot(gathered, w_in, preferred_element_type=jnp.float32).astype(jnp.bfloat16)
    mixer_act, state_next = state_mixer(
        u_in, state_prev, decay_rate, rotation, log_step, in_re, in_im, read_re, read_im, skip_gain
    )
    mixer_bf = mixer_act.astype(jnp.bfloat16)
    all_channels = lax.all_gather(mixer_bf, "tp", axis=1, tiled=True)
    glu_logit = jnp.dot(all_channels, w_glu, preferred_element_type=jnp.float32)
    mixed = (mixer_act * jax.nn.sigmoid(glu_logit)).astype(jnp.bfloat16)
    partial_out = jnp.dot(mixed, w_out, preferred_element_type=jnp.float32)
    branch = lax.psum_scatter(
        partial_out.astype(jnp.bfloat16), "tp", scatter_dimension=1, tiled=True
    ).astype(jnp.float32)
    after_float = (source + branch).astype(jnp.bfloat16).astype(jnp.float32)
    squares_ffn = lax.psum(jnp.sum(after_float * after_float, axis=1), "tp")
    ffn_own = lax.dynamic_slice_in_dim(ffn_gain, tp_place * shard_width, shard_width)
    scale_ffn = lax.rsqrt(squares_ffn / full_width + epsilon)[:, None]
    normed_ffn = (after_float * scale_ffn * ffn_own).astype(jnp.bfloat16)
    flat_routes = routes.reshape(-1)
    onehot = (flat_routes[:, None] == jnp.arange(experts_all, dtype=jnp.int32)).astype(jnp.int32)
    before = jnp.cumsum(onehot, axis=0) - onehot
    slot_index = jnp.sum(before * onehot, axis=1)
    destination = (flat_routes * capacity + slot_index).reshape(seq_rows, TOPK)
    matches = destination[:, :, None] == jnp.arange(experts_all * capacity, dtype=jnp.int32)
    dispatch_map = jnp.sum(matches.astype(jnp.float32), axis=1).astype(jnp.bfloat16)
    combine_map = jnp.sum(jnp.where(matches, route_weights[:, :, None], 0.0), axis=1)
    outbound = jnp.einsum("bj,bd->jd", dispatch_map, normed_ffn, preferred_element_type=jnp.float32)
    outbound = outbound.astype(jnp.bfloat16).reshape(experts_all, capacity, shard_width)
    arrived = lax.all_gather(
        lax.all_to_all(outbound, "ep", split_axis=0, concat_axis=0, tiled=True),
        "tp",
        axis=2,
        tiled=True,
    )
    sources, slots_here, row_width = arrived.shape
    flat_rows = arrived.reshape(sources * slots_here, row_width)
    gate_value = jnp.dot(flat_rows, w_gate[0], preferred_element_type=jnp.float32)
    up_value = jnp.dot(flat_rows, w_up[0], preferred_element_type=jnp.float32)
    hidden = (jax.nn.silu(gate_value) * up_value).astype(jnp.bfloat16)
    partial_sum = jnp.dot(hidden, w_down[0], preferred_element_type=jnp.float32)
    partial_sum = partial_sum.reshape(sources, slots_here, row_width)
    reduced = lax.psum_scatter(
        partial_sum.astype(jnp.bfloat16), "tp", scatter_dimension=2, tiled=True
    )
    came_back = lax.all_to_all(reduced, "ep", split_axis=0, concat_axis=0, tiled=True)
    came_back = came_back.reshape(experts_all * capacity, shard_width).astype(jnp.float32)
    combined = jnp.dot(combine_map, came_back, precision=highest)
    layer_out = (after_float + combined).astype(jnp.bfloat16)
    return (layer_out, state_next)


def solution(mesh):
    return jax.shard_map(
        per_device,
        mesh=mesh,
        in_specs=(
            P("ep", "tp"),
            P("ep", None),
            P("ep", None),
            P("ep", None, "tp", None),
            P(),
            P(),
            P(None, "tp"),
            P("tp", None),
            P("tp", None),
            P("tp"),
            P("tp", None, None),
            P("tp", None, None),
            P("tp", None, None),
            P("tp", None, None),
            P("tp", None),
            P(None, "tp"),
            P("tp", None),
            P("ep", None, "tp"),
            P("ep", None, "tp"),
            P("ep", "tp", None),
        ),
        out_specs=(P("ep", "tp"), P("ep", None, "tp", None)),
        check_vma=False,
    )
```

profile of v0, /device:TPU:0, one launch (start us, length us, event | category | flops | bytes accessed | tf_op | source)
XLA Modules:
  0.0 192.4 jit_solution(10713720667919204251)
XLA Ops:
  7.2 0.0 copy-start
  7.2 0.0 reduce-scatter.3.cloned.1.call-start
  7.2 0.8 exp.13
  8.0 1.0 fusion.25
  9.1 8.4 %psum.14 = f32[64]{0:T(128)S(1)} all-reduce(f32[64]{0:T(128)S(1)} %fusion.25), channel_id=1, replica_groups=mesh['ep'=8,'tp'=4] {'tp'}, use_global_device_ids=true, to_apply=%region_1.0 | all-reduce | flops 64 | bytes 512 | tf_op jit(solution)/shard_map/psum | solution.py:71
  17.5 0.7 dynamic_slice.6
  18.2 1.0 fusion.27
  19.2 6.5 %all_gather.9 = bf16[64,4096]{1,0:T(8,128)(2,1)S(1)} all-gather(bf16[64,1024]{1,0:T(8,128)(2,1)S(1)} %fusion.27), channel_id=1, replica_groups=mesh['ep'=8,'tp'=4] {'tp'}, dimensions={1}, use_global_device_ids=true | all-gather | bytes 655360 | tf_op jit(solution)/shard_map/all_gather | solution.py:75
  25.7 2.1 %convolution_convert_fusion.2 = bf16[64,256]{1,0:T(8,128)(2,1)S(1)} fusion(bf16[64,4096]{1,0:T(8,128)(2,1)S(1)} %all_gather.9, bf16[4096,256]{1,0:T(8,128)(2,1)} %param.26), kind=kOutput, calls=%fused_computation.26 | convolution fusion | flops 134234112 | bytes 2654208 | tf_op jit(solution)/shard_map/dot_general | solution.py:76
  27.8 0.1 copy.55
  27.9 1.3 fusion.62
  29.2 0.1 add_divide_fusion
  29.4 0.7 fusion.15
  30.1 0.7 fusion.16
  30.7 0.9 fusion.63
  31.7 0.9 fusion.19
  32.6 0.1 copy.60
  32.7 5.4 %all_gather.10 = bf16[64,1024]{1,0:T(8,128)(2,1)S(1)} all-gather(bf16[64,256]{1,0:T(8,128)(2,1)S(1)} %fusion.56), channel_id=1, replica_groups=mesh['ep'=8,'tp'=4] {'tp'}, dimensions={1}, use_global_device_ids=true | all-gather | bytes 163840 | tf_op jit(solution)/shard_map/all_gather | solution.py:81
  38.2 2.7 %convolution_convert_fusion = bf16[64,4096]{1,0:T(8,128)(2,1)} fusion(bf16[256,4096]{1,0:T(8,128)(2,1)S(1)} %copy-done, bf16[64,1024]{1,0:T(8,128)(2,1)S(1)} %all_gather.10, bf16[1024,256]{1,0:T(8,128)(2,1)} %param.35, f32[64,256]{1,0:T(8,128)S(1)} %copy.60), kind=kOutput, calls=%fused_computation.7 | convolution fusion | flops 168247296 | bytes 3342336 | tf_op jit(solution)/shard_map/dot_general | solution.py:84
  40.8 0.0 reduce-scatter.3.cloned.1.call-update
  40.9 0.0 all-gather.2.cloned.1.call-start
  40.9 0.1 copy.61
  41.0 0.1 eq.28
  41.2 0.1 fusion.48
  41.3 0.2 reduce_window_sum.11
  41.4 0.2 select_reduce_fusion.1
  41.6 0.1 reduce_sum.49
  41.8 0.1 copy.62
  41.8 0.1 convert_reduce_fusion
  42.0 21.7 %reduce-scatter.3.cloned.1.call-done = bf16[64,1024]{1,0:T(8,128)(2,1)} async-done(((bf16[64,4096]{1,0:T(8,128)(2,1)}), bf16[64,1024]{1,0:T(8,128)(2,1)}) %reduce-scatter.3.cloned.1.call-update) | async-done | bytes 131088 | tf_op jit(solution)/shard_map/reduce_scatter | solution.py:85
  63.6 1.0 fusion.29
  64.7 5.8 %psum.15 = f32[64]{0:T(128)S(1)} all-reduce(f32[64]{0:T(128)S(1)} %fusion.29), channel_id=1, replica_groups=mesh['ep'=8,'tp'=4] {'tp'}, use_global_device_ids=true, to_apply=%region_8.9 | all-reduce | flops 64 | bytes 512 | tf_op jit(solution)/shard_map/psum | solution.py:89
  70.5 1.2 convolution_convert_fusion.1
  71.7 19.8 %all_to_all.10 = bf16[8,32,1024]{2,1,0:T(8,128)(2,1)} all-to-all(bf16[8,32,1024]{2,1,0:T(8,128)(2,1)S(1)} %bitcast.67), channel_id=1, replica_groups=mesh['ep'=8,'tp'=4] {'ep'}, dimensions={0} | all-to-all | bytes 1048576 | tf_op jit(solution)/shard_map/all_to_all | solution.py:104
  91.6 0.0 all-gather.2.cloned.1.call-update
  91.6 0.0 reduce-scatter.5.cloned.1.call-start
  91.6 20.8 %all-gather.2.cloned.1.call-done = bf16[8,32,4096]{2,1,0:T(8,128)(2,1)} async-done(((bf16[8,32,1024]{2,1,0:T(8,128)(2,1)}), bf16[8,32,4096]{2,1,0:T(8,128)(2,1)}) %all-gather.2.cloned.1.call-update) | async-done | bytes 2097168 | tf_op jit(solution)/shard_map/all_gather | solution.py:103
  112.4 7.4 %fusion.4 = f32[256,1408]{1,0:T(8,128)S(1)} fusion(bf16[256,4096]{1,0:T(8,128)(2,1)} %bitcast.74, bf16[1,4096,1408]{2,1,0:T(8,128)(2,1)} %param.37), kind=kOutput, calls=%fused_computation.4 | convolution fusion | flops 2952790016 | bytes 15073280 | tf_op jit(solution)/shard_map/dot_general | solution.py:111
  119.9 0.0 slice-start.2
  119.9 8.0 %fusion.12 = bf16[256,1408]{1,0:T(8,128)(2,1)S(1)} fusion(bf16[256,4096]{1,0:T(8,128)(2,1)S(1)} %bitcast.75, bf16[1,4096,1408]{2,1,0:T(8,128)(2,1)} %param.38, f32[256,1408]{1,0:T(8,128)S(1)} %fusion.4), kind=kOutput, calls=%fused_computation.9 | convolution fusion | flops 2954952704 | bytes 15794176 | tf_op jit(solution)/shard_map/dot_general | solution.py:112
  127.9 4.6 %fusion.6 = bf16[8,32,4096]{2,1,0:T(8,128)(2,1)} fusion(bf16[8,32,1408]{2,1,0:T(8,128)(2,1)S(1)} %bitcast.76, bf16[1,1408,4096]{2,1,0:T(8,128)(2,1)S(1)} %bitcast.73), kind=kOutput, calls=%fused_computation.6 | convolution fusion | flops 2953838592 | bytes 14352384 | tf_op jit(solution)/shard_map/dot_general | solution.py:114
  132.5 0.0 reduce-scatter.5.cloned.1.call-update
  132.6 31.3 %reduce-scatter.5.cloned.1.call-done = bf16[8,32,1024]{2,1,0:T(8,128)(2,1)} async-done(((bf16[8,32,4096]{2,1,0:T(8,128)(2,1)}), bf16[8,32,1024]{2,1,0:T(8,128)(2,1)}) %reduce-scatter.5.cloned.1.call-update) | async-done | bytes 524304 | tf_op jit(solution)/shard_map/reduce_scatter | solution.py:116
  163.9 5.5 %all-to-all-start.1 = ((bf16[8,32,1024]{2,1,0:T(8,128)(2,1)}), bf16[8,32,1024]{2,1,0:T(8,128)(2,1)}, u32[]{:S(2)}, u32[]{:S(2)}) async-start(bf16[8,32,1024]{2,1,0:T(8,128)(2,1)} %reduce-scatter.5.cloned.1.call-done), calls=%async_computation.3 | async-start | bytes 1048576 | tf_op jit(solution)/shard_map/all_to_all | solution.py:119
  169.4 0.1 pad_maximum_fusion
  169.5 1.6 copy.63
  171.1 12.7 %all-to-all-done.1 = bf16[8,32,1024]{2,1,0:T(8,128)(2,1)} async-done(((bf16[8,32,1024]{2,1,0:T(8,128)(2,1)}), bf16[8,32,1024]{2,1,0:T(8,128)(2,1)}, u32[]{:S(2)}, u32[]{:S(2)}) %all-to-all-start.1) | async-done | bytes 524320 | tf_op jit(solution)/shard_map/all_to_all | solution.py:119
  183.8 2.1 %fusion.17 = bf16[64,1024]{1,0:T(8,128)(2,1)} fusion(f32[64,256]{1,0:T(8,128)S(1)} %get-tuple-element.11, bf16[256,1024]{1,0:T(8,128)(2,1)} %bitcast.14, bf16[64,1024]{1,0:T(8,128)(2,1)S(1)} %copy-done.2, bf16[64,1024]{1,0:T(8,128)(2,1)S(1)} %copy-done.1), kind=kOutput, calls=%fused_computation.16 | convolution fusion | flops 201785344 | bytes 983040 | tf_op jit(solution)/shard_map/dot_general | solution.py:121
  (37 shorter events, 0.1 us)
Async XLA Ops:
  7.2 31.0 %copy-start = (bf16[256,4096]{1,0:T(8,128)(2,1)S(1)}, bf16[256,4096]{1,0:T(8,128)(2,1)}, u32[]{:S(2)}) copy-start(bf16[256,4096]{1,0:T(8,128)(2,1)} %param.36) | copy-start | bytes 6291460
  7.2 56.5 %reduce-scatter.3.cloned.1.call-start = ((), (), s32[]{:S(2)}) async-start(), calls=%async_computation.4 | async-start | bytes 655360 | tf_op jit(solution)/shard_map/reduce_scatter | solution.py:85
  25.7 3.5 %copy-start.8 = (f32[16,64]{1,0:T(8,128)S(1)}, f32[16,64]{1,0:T(8,128)}, u32[]{:S(2)}) copy-start(f32[16,64]{1,0:T(8,128)} %param.28) | copy-start | bytes 12292
  25.7 3.5 %copy-start.9 = (f32[16,64]{1,0:T(8,128)S(1)}, f32[16,64]{1,0:T(8,128)}, u32[]{:S(2)}) copy-start(f32[16,64]{1,0:T(8,128)} %param.27) | copy-start | bytes 12292
  25.7 3.7 %copy-start.3 = (f32[16,64,16]{1,2,0:T(8,128)S(1)}, f32[16,64,16]{1,2,0:T(8,128)}, u32[]{:S(2)}) copy-start(f32[16,64,16]{1,2,0:T(8,128)} %param.31) | copy-start | bytes 196612
  25.7 3.7 %copy-start.4 = (f32[16,64,16]{1,2,0:T(8,128)S(1)}, f32[16,64,16]{1,2,0:T(8,128)}, u32[]{:S(2)}) copy-start(f32[16,64,16]{1,2,0:T(8,128)} %param.30) | copy-start | bytes 196612
  29.2 1.5 copy-start.6
  29.4 2.3 %copy-start.5 = (f32[16,16,64]{2,1,0:T(8,128)S(1)}, f32[16,16,64]{2,1,0:T(8,128)}, u32[]{:S(2)}) copy-start(f32[16,16,64]{2,1,0:T(8,128)} %param.33) | copy-start | bytes 196612
  29.4 2.3 %copy-start.7 = (f32[16,16]{1,0:T(8,128)S(1)}, f32[16,16]{1,0:T(8,128)}, u32[]{:S(2)}) copy-start(f32[16,16]{1,0:T(8,128)} %param.34) | copy-start | bytes 3076
  32.7 8.2 %copy-start.10 = (s32[64,2]{0,1:T(2,128)S(1)}, s32[64,2]{0,1:T(2,128)}, u32[]{:S(2)}) copy-start(s32[64,2]{0,1:T(2,128)} %param.21) | copy-start | bytes 1540
  38.2 3.7 %copy-start.11 = (f32[64,2]{0,1:T(2,128)S(1)}, f32[64,2]{0,1:T(2,128)}, u32[]{:S(2)}) copy-start(f32[64,2]{0,1:T(2,128)} %param.22) | copy-start | bytes 1540
  38.2 25.5 %copy-start.1 = (bf16[64,1024]{1,0:T(8,128)(2,1)S(1)}, bf16[64,1024]{1,0:T(8,128)(2,1)}, u32[]{:S(2)}) copy-start(bf16[64,1024]{1,0:T(8,128)(2,1)} %param.20) | copy-start | bytes 393220
  38.2 32.3 %dynamic-slice-start = ((f32[4096]{0:T(1024)}, s32[]{:T(128)}), f32[1024]{0:T(1024)S(1)}, s32[]{:S(2)}) async-start(f32[4096]{0:T(1024)} %param.25, s32[]{:T(128)} %select_n.8), calls=%async_computation.7 | async-start | bytes 8704 | tf_op jit(solution)/shard_map/dynamic_slice | solution.py:90
  40.9 71.6 %all-gather.2.cloned.1.call-start = ((), (), s32[]{:S(2)}) async-start(), calls=%async_computation.5 | async-start | bytes 2621440 | tf_op jit(solution)/shard_map/all_gather | solution.py:103
  91.6 72.3 %reduce-scatter.5.cloned.1.call-start = ((), (), s32[]{:S(2)}) async-start(), calls=%async_computation.6 | async-start | bytes 2621440 | tf_op jit(solution)/shard_map/reduce_scatter | solution.py:116
  112.4 7.4 %copy-start.12 = (bf16[8,32,4096]{2,1,0:T(8,128)(2,1)S(1)}, bf16[8,32,4096]{2,1,0:T(8,128)(2,1)}, u32[]{:S(2)}) copy-start(bf16[8,32,4096]{2,1,0:T(8,128)(2,1)} %all-gather.2.cloned.1.call-done) | copy-start | bytes 6291460
  112.4 15.5 %slice-start = ((s8[11534336]{0:T(1024)(128)(4,1)}), s8[4194304]{0:T(1024)(128)(4,1)S(1)}, s32[]{:S(2)}) async-start(s8[11534336]{0:T(1024)(128)(4,1)} %bitcast.72), calls=%async_computation.8 | async-start | bytes 8388608
  112.4 15.5 %slice-start.1 = ((s8[11534336]{0:T(1024)(128)(4,1)}), s8[4194304]{0:T(1024)(128)(4,1)S(1)}, s32[]{:S(2)}) async-start(s8[11534336]{0:T(1024)(128)(4,1)} %bitcast.72), calls=%async_computation.9 | async-start | bytes 8388608
  119.9 8.0 %slice-start.2 = ((s8[11534336]{0:T(1024)(128)(4,1)}), s8[3145728]{0:T(1024)(128)(4,1)S(1)}, s32[]{:S(2)}) async-start(s8[11534336]{0:T(1024)(128)(4,1)} %bitcast.72), calls=%async_computation.10 | async-start | bytes 6291456
  163.9 19.9 %all-to-all-start.1 = ((bf16[8,32,1024]{2,1,0:T(8,128)(2,1)}), bf16[8,32,1024]{2,1,0:T(8,128)(2,1)}, u32[]{:S(2)}, u32[]{:S(2)}) async-start(bf16[8,32,1024]{2,1,0:T(8,128)(2,1)} %reduce-scatter.5.cloned.1.call-done), calls=%async_computation.3 | async-start | bytes 1048576 | tf_op jit(solution)/shard_map/all_to_all | solution.py:119
  169.4 14.4 %copy-start.2 = (bf16[64,1024]{1,0:T(8,128)(2,1)S(1)}, bf16[64,1024]{1,0:T(8,128)(2,1)}, u32[]{:S(2)}) copy-start(bf16[64,1024]{1,0:T(8,128)(2,1)} %reduce-scatter.3.cloned.1.call-done) | copy-start | bytes 393220
Sparse Core Ops, SparseCore 0:
  41.0 22.5 reduce-scatter.2
  91.7 20.6 all-gather.1
  132.7 31.1 reduce-scatter.4
where the time goes:
time: 193 us; the launch traced here: 192 us
  waiting for transfers between devices  86.5 us (45%)
  blocking collectives  45.9 us (24%)
  matrix products  31.3 us (16%)
  between operations  14 us (7%)
  starting transfers between devices  5.63 us (3%)
  local copies, waits for them, and re-layouts  5.09 us (3%)
  other arithmetic  3.92 us (2%)
    reduce_scatter x1, waiting for transfers between devices, per_device(): lax.psum_scatter(partial_sum.astype(jnp.bfloat16), 'tp', scatter_dimensio...  31.3 us
    reduce_scatter x1, waiting for transfers between devices, per_device(): lax.psum_scatter(partial_out.astype(jnp.bfloat16), 'tp', scatter_dimensio...  21.7 us
    all_gather x1, waiting for transfers between devices, per_device(): lax.all_gather(lax.all_to_all(outbound, 'ep', split_axis=0, concat_axis=0...  20.8 us
    all_to_all x1, blocking collectives, per_device(): lax.all_to_all(outbound, 'ep', split_axis=0, concat_axis=0, tiled=True)  19.8 us
    all_to_all x1, waiting for transfers between devices, per_device(): lax.all_to_all(reduced, 'ep', split_axis=0, concat_axis=0, tiled=True)  12.7 us
    psum x1, blocking collectives, per_device(): squares = lax.psum(jnp.sum(source * source, axis=1), 'tp')  8.4 us
    dot_general x1, matrix products, per_device(): up_value = jnp.dot(flat_rows, w_up[0], preferred_element_type=jnp.float32)  8.01 us
    dot_general x1, matrix products, per_device(): jnp.dot(flat_rows, w_gate[0], preferred_element_type=jnp.float32)  7.42 us
  transfers between devices with their start and end apart: 4, of which 4 were waited for; matrix products, arithmetic and copies ran while one was open for 1% of the time, Pallas kernels for 0%

commit v1 on v0

--- a/solution.py
+++ b/solution.py
@@ -100,12 +100,9 @@
     combine_map = jnp.sum(jnp.where(matches, route_weights[:, :, None], 0.0), axis=1)
     outbound = jnp.einsum("bj,bd->jd", dispatch_map, normed_ffn, preferred_element_type=jnp.float32)
     outbound = outbound.astype(jnp.bfloat16).reshape(experts_all, capacity, shard_width)
-    arrived = lax.all_gather(
-        lax.all_to_all(outbound, "ep", split_axis=0, concat_axis=0, tiled=True),
-        "tp",
-        axis=2,
-        tiled=True,
-    )
+    block = lax.all_to_all(outbound, "ep", split_axis=0, concat_axis=0, tiled=True)
+    parts = lax.all_gather(block, "tp", axis=0, tiled=False)
+    arrived = jnp.concatenate(parts, axis=2)
     sources, slots_here, row_width = arrived.shape
     flat_rows = arrived.reshape(sources * slots_here, row_width)
     gate_value = jnp.dot(flat_rows, w_gate[0], preferred_element_type=jnp.float32)

time: 193 us -> 192 us (level)
  matrix products: 31.3 us -> 26.2 us
  local copies, waits for them, and re-layouts: 5.09 us -> 9.41 us
    dot_general x1, matrix products: 8.01 us -> 3.5 us  [per_device(): up_value = jnp.dot(flat_rows, w_up[0], preferred_element_type=jnp.float32)]
    reshape x0 -> x1, local copies, waits for them, and re-layouts: none -> 3.22 us  [per_device(): arrived = jnp.concatenate(parts, axis=2)]
where the time goes in v1:
time: 192 us
  waiting for transfers between devices  86.4 us (45%)
  blocking collectives  45.9 us (24%)
  matrix products  26.2 us (14%)
  between operations  14.1 us (7%)
  local copies, waits for them, and re-layouts  9.41 us (5%)
  starting transfers between devices  5.81 us (3%)
  other arithmetic  3.92 us (2%)
    reduce_scatter x1, waiting for transfers between devices, per_device(): lax.psum_scatter(partial_sum.astype(jnp.bfloat16), 'tp', scatter_dimensio...  31.3 us
    reduce_scatter x1, waiting for transfers between devices, per_device(): lax.psum_scatter(partial_out.astype(jnp.bfloat16), 'tp', scatter_dimensio...  21.7 us
    all_gather x1, waiting for transfers between devices, per_device(): parts = lax.all_gather(block, 'tp', axis=0, tiled=False)  20.6 us
    all_to_all x1, blocking collectives, per_device(): lax.all_to_all(outbound, 'ep', split_axis=0, concat_axis=0, tiled=True)  19.8 us
    all_to_all x1, waiting for transfers between devices, per_device(): lax.all_to_all(reduced, 'ep', split_axis=0, concat_axis=0, tiled=True)  12.7 us
    psum x1, blocking collectives, per_device(): squares = lax.psum(jnp.sum(source * source, axis=1), 'tp')  8.4 us
    dot_general x1, matrix products, per_device(): jnp.dot(flat_rows, w_gate[0], preferred_element_type=jnp.float32)  6.73 us
    all_gather x1, blocking collectives, per_device(): gathered = lax.all_gather(outgoing, 'tp', axis=1, tiled=True)  6.5 us
  transfers between devices with their start and end apart: 4, of which 4 were waited for; matrix products, arithmetic and copies ran while one was open for 1% of the time, Pallas kernels for 0%

profile of v1, /device:TPU:0, one launch (start us, length us, event | category | flops | bytes accessed | tf_op | source)
XLA Modules:
  0.0 191.7 jit_solution(4413990284348459242)
XLA Ops:
  7.2 0.0 reduce-scatter.3.cloned.1.call-start
  7.2 0.8 exp.13
  8.0 1.0 fusion.25
  9.1 8.4 %psum.14 = f32[64]{0:T(128)S(1)} all-reduce(f32[64]{0:T(128)S(1)} %fusion.25), channel_id=1, replica_groups=mesh['ep'=8,'tp'=4] {'tp'}, use_global_device_ids=true, to_apply=%region_1.0 | all-reduce | flops 64 | bytes 512 | tf_op jit(solution)/shard_map/psum | solution.py:71
  17.5 0.7 dynamic_slice.6
  18.2 1.0 fusion.27
  19.2 6.5 %all_gather.12 = bf16[64,4096]{1,0:T(8,128)(2,1)S(1)} all-gather(bf16[64,1024]{1,0:T(8,128)(2,1)S(1)} %fusion.27), channel_id=1, replica_groups=mesh['ep'=8,'tp'=4] {'tp'}, dimensions={1}, use_global_device_ids=true | all-gather | bytes 655360 | tf_op jit(solution)/shard_map/all_gather | solution.py:75
  25.7 2.1 %convolution_convert_fusion.2 = bf16[64,256]{1,0:T(8,128)(2,1)S(1)} fusion(bf16[64,4096]{1,0:T(8,128)(2,1)S(1)} %all_gather.12, bf16[4096,256]{1,0:T(8,128)(2,1)} %param.26), kind=kOutput, calls=%fused_computation.26 | convolution fusion | flops 134234112 | bytes 2654208 | tf_op jit(solution)/shard_map/dot_general | solution.py:76
  27.8 0.1 copy.84
  27.9 1.3 fusion.62
  29.2 0.1 add_divide_fusion
  29.4 0.7 fusion.15
  30.1 0.7 fusion.16
  30.7 0.9 fusion.63
  31.7 0.9 fusion.19
  32.6 0.1 copy.89
  32.8 5.4 %all_gather.13 = bf16[64,1024]{1,0:T(8,128)(2,1)S(1)} all-gather(bf16[64,256]{1,0:T(8,128)(2,1)S(1)} %fusion.56), channel_id=1, replica_groups=mesh['ep'=8,'tp'=4] {'tp'}, dimensions={1}, use_global_device_ids=true | all-gather | bytes 163840 | tf_op jit(solution)/shard_map/all_gather | solution.py:81
  38.2 2.7 %convolution_convert_fusion = bf16[64,4096]{1,0:T(8,128)(2,1)} fusion(bf16[256,4096]{1,0:T(8,128)(2,1)S(1)} %copy-done, bf16[64,1024]{1,0:T(8,128)(2,1)S(1)} %all_gather.13, bf16[1024,256]{1,0:T(8,128)(2,1)} %param.35, f32[64,256]{1,0:T(8,128)S(1)} %copy.89), kind=kOutput, calls=%fused_computation.7 | convolution fusion | flops 168247296 | bytes 3342336 | tf_op jit(solution)/shard_map/dot_general | solution.py:84
  40.9 0.0 reduce-scatter.3.cloned.1.call-update
  40.9 0.0 all-gather.3.cloned.1.call-start
  40.9 0.1 copy.90
  41.0 0.1 eq.28
  41.2 0.1 fusion.48
  41.3 0.2 reduce_window_sum.11
  41.4 0.2 select_reduce_fusion.1
  41.6 0.1 reduce_sum.49
  41.8 0.1 copy.91
  41.8 0.1 convert_reduce_fusion
  42.0 21.7 %reduce-scatter.3.cloned.1.call-done = bf16[64,1024]{1,0:T(8,128)(2,1)} async-done(((bf16[64,4096]{1,0:T(8,128)(2,1)}), bf16[64,1024]{1,0:T(8,128)(2,1)}) %reduce-scatter.3.cloned.1.call-update) | async-done | bytes 131088 | tf_op jit(solution)/shard_map/reduce_scatter | solution.py:85
  63.6 1.0 fusion.29
  64.7 5.8 %psum.15 = f32[64]{0:T(128)S(1)} all-reduce(f32[64]{0:T(128)S(1)} %fusion.29), channel_id=1, replica_groups=mesh['ep'=8,'tp'=4] {'tp'}, use_global_device_ids=true, to_apply=%region_8.9 | all-reduce | flops 64 | bytes 512 | tf_op jit(solution)/shard_map/psum | solution.py:89
  70.5 1.3 convolution_convert_fusion.1
  71.7 19.8 %all_to_all.10 = bf16[8,32,1024]{2,1,0:T(8,128)(2,1)} all-to-all(bf16[8,32,1024]{2,1,0:T(8,128)(2,1)S(1)} %bitcast.76), channel_id=1, replica_groups=mesh['ep'=8,'tp'=4] {'ep'}, dimensions={0} | all-to-all | bytes 1048576 | tf_op jit(solution)/shard_map/all_to_all | solution.py:103
  91.5 0.0 all-gather.3.cloned.1.call-update
  91.6 0.2 reduce-scatter.5.cloned.1.call-start
  91.8 20.6 %all-gather.3.cloned.1.call-done = bf16[32,32,1024]{2,1,0:T(8,128)(2,1)} async-done(((bf16[8,32,1024]{2,1,0:T(8,128)(2,1)}), bf16[32,32,1024]{2,1,0:T(8,128)(2,1)}) %all-gather.3.cloned.1.call-update) | async-done | bytes 2097168 | tf_op jit(solution)/shard_map/all_gather | solution.py:104
  112.4 3.2 %copy.92 = bf16[8,32,4,1024]{3,2,1,0:T(4,128)(2,1)S(1)} copy(bf16[8,32,4,1024]{3,1,0,2:T(8,128)(2,1)} %bitcast.73) | data formatting | bytes 4194304 | tf_op jit(solution)/shard_map/reshape | solution.py:105
  115.7 0.9 copy.96
  116.6 6.7 %fusion.4 = f32[256,1408]{1,0:T(8,128)S(1)} fusion(bf16[256,4096]{1,0:T(8,128)(2,1)S(1)} %bitcast.74, bf16[1,4096,1408]{2,1,0:T(8,128)(2,1)} %param.37), kind=kOutput, calls=%fused_computation.4 | convolution fusion | flops 2952790016 | bytes 15073280 | tf_op jit(solution)/shard_map/dot_general | solution.py:108
  123.3 0.2 slice-done.2
  123.6 3.5 %fusion.12 = bf16[256,1408]{1,0:T(8,128)(2,1)S(1)} fusion(bf16[256,4096]{1,0:T(8,128)(2,1)S(1)} %bitcast.75, bf16[1,4096,1408]{2,1,0:T(8,128)(2,1)S(1)} %bitcast.82, f32[256,1408]{1,0:T(8,128)S(1)} %fusion.4), kind=kOutput, calls=%fused_computation.9 | convolution fusion | flops 2954952704 | bytes 15794176 | tf_op jit(solution)/shard_map/dot_general | solution.py:109
  127.1 4.7 %fusion.6 = bf16[8,32,4096]{2,1,0:T(8,128)(2,1)} fusion(bf16[8,32,1408]{2,1,0:T(8,128)(2,1)S(1)} %bitcast.85, bf16[1,1408,4096]{2,1,0:T(8,128)(2,1)S(1)} %bitcast.84), kind=kOutput, calls=%fused_computation.6 | convolution fusion | flops 2953838592 | bytes 14352384 | tf_op jit(solution)/shard_map/dot_general | solution.py:111
  131.8 31.3 %reduce-scatter.5.cloned.1.call-done = bf16[8,32,1024]{2,1,0:T(8,128)(2,1)} async-done(((bf16[8,32,4096]{2,1,0:T(8,128)(2,1)}), bf16[8,32,1024]{2,1,0:T(8,128)(2,1)}) %reduce-scatter.5.cloned.1.call-update) | async-done | bytes 524304 | tf_op jit(solution)/shard_map/reduce_scatter | solution.py:113
  163.1 5.5 %all-to-all-start.1 = ((bf16[8,32,1024]{2,1,0:T(8,128)(2,1)}), bf16[8,32,1024]{2,1,0:T(8,128)(2,1)}, u32[]{:S(2)}, u32[]{:S(2)}) async-start(bf16[8,32,1024]{2,1,0:T(8,128)(2,1)} %reduce-scatter.5.cloned.1.call-done), calls=%async_computation.3 | async-start | bytes 1048576 | tf_op jit(solution)/shard_map/all_to_all | solution.py:116
  168.6 0.1 pad_maximum_fusion
  168.8 1.6 copy.93
  170.3 12.7 %all-to-all-done.1 = bf16[8,32,1024]{2,1,0:T(8,128)(2,1)} async-done(((bf16[8,32,1024]{2,1,0:T(8,128)(2,1)}), bf16[8,32,1024]{2,1,0:T(8,128)(2,1)}, u32[]{:S(2)}, u32[]{:S(2)}) %all-to-all-start.1) | async-done | bytes 524320 | tf_op jit(solution)/shard_map/all_to_all | solution.py:116
  183.1 2.1 %fusion.17 = bf16[64,1024]{1,0:T(8,128)(2,1)} fusion(f32[64,256]{1,0:T(8,128)S(1)} %get-tuple-element.15, bf16[256,1024]{1,0:T(8,128)(2,1)} %bitcast.15, bf16[64,1024]{1,0:T(8,128)(2,1)S(1)} %copy-done.2, bf16[64,1024]{1,0:T(8,128)(2,1)S(1)} %copy-done.1), kind=kOutput, calls=%fused_computation.16 | convolution fusion | flops 201785344 | bytes 983040 | tf_op jit(solution)/shard_map/dot_general | solution.py:118
  (44 shorter events, 0.2 us)
Async XLA Ops:
  7.2 31.0 %copy-start = (bf16[256,4096]{1,0:T(8,128)(2,1)S(1)}, bf16[256,4096]{1,0:T(8,128)(2,1)}, u32[]{:S(2)}) copy-start(bf16[256,4096]{1,0:T(8,128)(2,1)} %param.36) | copy-start | bytes 6291460
  7.2 56.5 %reduce-scatter.3.cloned.1.call-start = ((), (), s32[]{:S(2)}) async-start(), calls=%async_computation.4 | async-start | bytes 655360 | tf_op jit(solution)/shard_map/reduce_scatter | solution.py:85
  25.7 3.5 %copy-start.8 = (f32[16,64]{1,0:T(8,128)S(1)}, f32[16,64]{1,0:T(8,128)}, u32[]{:S(2)}) copy-start(f32[16,64]{1,0:T(8,128)} %param.28) | copy-start | bytes 12292
  25.7 3.5 %copy-start.9 = (f32[16,64]{1,0:T(8,128)S(1)}, f32[16,64]{1,0:T(8,128)}, u32[]{:S(2)}) copy-start(f32[16,64]{1,0:T(8,128)} %param.27) | copy-start | bytes 12292
  25.7 3.7 %copy-start.3 = (f32[16,64,16]{1,2,0:T(8,128)S(1)}, f32[16,64,16]{1,2,0:T(8,128)}, u32[]{:S(2)}) copy-start(f32[16,64,16]{1,2,0:T(8,128)} %param.31) | copy-start | bytes 196612
  25.7 3.7 %copy-start.4 = (f32[16,64,16]{1,2,0:T(8,128)S(1)}, f32[16,64,16]{1,2,0:T(8,128)}, u32[]{:S(2)}) copy-start(f32[16,64,16]{1,2,0:T(8,128)} %param.30) | copy-start | bytes 196612
  29.2 1.5 copy-start.6
  29.4 2.3 %copy-start.5 = (f32[16,16,64]{2,1,0:T(8,128)S(1)}, f32[16,16,64]{2,1,0:T(8,128)}, u32[]{:S(2)}) copy-start(f32[16,16,64]{2,1,0:T(8,128)} %param.33) | copy-start | bytes 196612
  29.4 2.3 %copy-start.7 = (f32[16,16]{1,0:T(8,128)S(1)}, f32[16,16]{1,0:T(8,128)}, u32[]{:S(2)}) copy-start(f32[16,16]{1,0:T(8,128)} %param.34) | copy-start | bytes 3076
  32.7 8.2 %copy-start.10 = (s32[64,2]{0,1:T(2,128)S(1)}, s32[64,2]{0,1:T(2,128)}, u32[]{:S(2)}) copy-start(s32[64,2]{0,1:T(2,128)} %param.21) | copy-start | bytes 1540
  38.2 3.7 %copy-start.11 = (f32[64,2]{0,1:T(2,128)S(1)}, f32[64,2]{0,1:T(2,128)}, u32[]{:S(2)}) copy-start(f32[64,2]{0,1:T(2,128)} %param.22) | copy-start | bytes 1540
  38.2 25.5 %copy-start.1 = (bf16[64,1024]{1,0:T(8,128)(2,1)S(1)}, bf16[64,1024]{1,0:T(8,128)(2,1)}, u32[]{:S(2)}) copy-start(bf16[64,1024]{1,0:T(8,128)(2,1)} %param.20) | copy-start | bytes 393220
  38.2 32.3 %dynamic-slice-start = ((f32[4096]{0:T(1024)}, s32[]{:T(128)}), f32[1024]{0:T(1024)S(1)}, s32[]{:S(2)}) async-start(f32[4096]{0:T(1024)} %param.25, s32[]{:T(128)} %select_n.8), calls=%async_computation.7 | async-start | bytes 8704 | tf_op jit(solution)/shard_map/dynamic_slice | solution.py:90
  40.9 71.5 %all-gather.3.cloned.1.call-start = ((), (), s32[]{:S(2)}) async-start(), calls=%async_computation.6 | async-start | bytes 2621440 | tf_op jit(solution)/shard_map/all_gather | solution.py:104
  91.6 71.6 %reduce-scatter.5.cloned.1.call-start = ((), (), s32[]{:S(2)}) async-start(), calls=%async_computation.5 | async-start | bytes 2621440 | tf_op jit(solution)/shard_map/reduce_scatter | solution.py:113
  115.6 7.7 %slice-start = ((s8[11534336]{0:T(1024)(128)(4,1)}), s8[4194304]{0:T(1024)(128)(4,1)S(1)}, s32[]{:S(2)}) async-start(s8[11534336]{0:T(1024)(128)(4,1)} %bitcast.81), calls=%async_computation.8 | async-start | bytes 8388608
  116.5 6.8 %slice-start.1 = ((s8[11534336]{0:T(1024)(128)(4,1)}), s8[4194304]{0:T(1024)(128)(4,1)S(1)}, s32[]{:S(2)}) async-start(s8[11534336]{0:T(1024)(128)(4,1)} %bitcast.81), calls=%async_computation.9 | async-start | bytes 8388608
  116.5 7.0 %slice-start.2 = ((s8[11534336]{0:T(1024)(128)(4,1)}), s8[3145728]{0:T(1024)(128)(4,1)S(1)}, s32[]{:S(2)}) async-start(s8[11534336]{0:T(1024)(128)(4,1)} %bitcast.81), calls=%async_computation.10 | async-start | bytes 6291456
  116.6 10.5 %slice-start.3 = ((s8[11534336]{0:T(1024)(128)(4,1)}), s8[4194304]{0:T(1024)(128)(4,1)S(1)}, s32[]{:S(2)}) async-start(s8[11534336]{0:T(1024)(128)(4,1)} %bitcast.83), calls=%async_computation.11 | async-start | bytes 8388608
  116.6 10.5 %slice-start.4 = ((s8[11534336]{0:T(1024)(128)(4,1)}), s8[4194304]{0:T(1024)(128)(4,1)S(1)}, s32[]{:S(2)}) async-start(s8[11534336]{0:T(1024)(128)(4,1)} %bitcast.83), calls=%async_computation.12 | async-start | bytes 8388608
  123.6 3.5 %slice-start.5 = ((s8[11534336]{0:T(1024)(128)(4,1)}), s8[3145728]{0:T(1024)(128)(4,1)S(1)}, s32[]{:S(2)}) async-start(s8[11534336]{0:T(1024)(128)(4,1)} %bitcast.83), calls=%async_computation.13 | async-start | bytes 6291456
  163.1 19.9 %all-to-all-start.1 = ((bf16[8,32,1024]{2,1,0:T(8,128)(2,1)}), bf16[8,32,1024]{2,1,0:T(8,128)(2,1)}, u32[]{:S(2)}, u32[]{:S(2)}) async-start(bf16[8,32,1024]{2,1,0:T(8,128)(2,1)} %reduce-scatter.5.cloned.1.call-done), calls=%async_computation.3 | async-start | bytes 1048576 | tf_op jit(solution)/shard_map/all_to_all | solution.py:116
  168.6 14.4 %copy-start.2 = (bf16[64,1024]{1,0:T(8,128)(2,1)S(1)}, bf16[64,1024]{1,0:T(8,128)(2,1)}, u32[]{:S(2)}) copy-start(bf16[64,1024]{1,0:T(8,128)(2,1)} %reduce-scatter.3.cloned.1.call-done) | copy-start | bytes 393220
Sparse Core Ops, SparseCore 0:
  41.0 22.5 reduce-scatter.2
  91.7 20.6 all-gather.2
  131.9 31.1 reduce-scatter.4
